TPU v7x, 256 devices: a whole 4x4x8 slice. The times are simulated.
256 devices in a mesh: ep: 64 (over z, y, core), tp: 4 (over x).
Axes of the slice: x: 4, y: 4, z: 8, core: 2. Of those that a mesh axis runs over, the one named last changes fastest.
Arguments:
- tokens: bfloat16 [1536, 1024], P('ep'), may hold values from -1.796875 to 1.796875
- attn_gain: float32 [1024], replicated, may hold values from 0.1 to 1.9
- w_query: bfloat16 [1024, 1024], P(None, 'tp'), may hold values from -0.1875 to 0.1875
- w_key: bfloat16 [1024, 256], P(None, 'tp'), may hold values from -0.1875 to 0.1875
- w_value: bfloat16 [1024, 256], P(None, 'tp'), may hold values from -0.1875 to 0.1875
- w_forget: bfloat16 [1024, 4], P(None, 'tp'), may hold values from -0.1875 to 0.1875
- forget_bias: float32 [4], P('tp'), may hold values from -1 to 2
- query_gain: float32 [64], replicated, may hold values from 0.1 to 1.9
- key_gain: float32 [64], replicated, may hold values from 0.1 to 1.9
- cache_pairs: bfloat16 [1536, 4, 1024, 128], P('ep', 'tp'), may hold values from -6 to 206
- cache_cum: float32 [1536, 4, 1024], P('ep', 'tp'), may hold values from -1024 to 0, as said below
- lengths: int32 [1536], P('ep'), may hold values from 64 to 1024, as said below
- w_output: bfloat16 [1024, 1024], P('tp'), may hold values from -0.1875 to 0.1875
- ffn_gain: float32 [1024], replicated, may hold values from 0.1 to 1.9
- expert_ids: int32 [1536, 2], replicated, may hold values from 0 to 63, all different within a row; in each aligned block of 24 rows (0 to 23, 24 to 47, ...) at most 2 rows name the same one
- route_weight: float32 [1536, 2], replicated, may hold values from 0.2 to 1
- w_exp_gate: bfloat16 [64, 1024, 3584], P('ep', None, 'tp'), may hold values from -0.1875 to 0.1875
- w_exp_up: bfloat16 [64, 1024, 3584], P('ep', None, 'tp'), may hold values from -0.1875 to 0.1875
- w_exp_down: bfloat16 [64, 3584, 1024], P('ep', 'tp'), may hold values from -0.09375 to 0.09375
- shared_gate: bfloat16 [1024], replicated, may hold values from -0.1875 to 0.1875
- w_dense_gate: bfloat16 [4096, 1024], P('ep'), may hold values from -0.1875 to 0.1875
- w_dense_up: bfloat16 [4096, 1024], P('ep'), may hold values from -0.1875 to 0.1875
- w_dense_down: bfloat16 [4096, 1024], P('ep', 'tp'), may hold values from -0.09375 to 0.09375
Outputs:
- layer_out: bfloat16 [1536, 1024], P('ep', 'tp')
Inputs may be any that keep to these rules, and one draw needn't show every extreme that they name: The cache of sequence b holds positions 0 to lengths[b] - 1; some sequence has 1024. `expert_ids`: each row names 2 different experts; in each aligned block of 24 rows no expert is named by more than 2 rows. cache_cum[b, g, s] never rises with s.
All inputs are finite; a program needn't handle non-finite values.
Results may differ from a plain program's by a relative error of at most 0.02.
Values may be sent and summed in bfloat16 or wider, within the bound.
A program may use at most 64 MiB of HBM per device.

v0:
```python
import jax
import jax.numpy as jnp
from jax import lax
from jax.sharding import Mesh
from jax.sharding import PartitionSpec as P

EP = ("ep_0", "ep_1", "ep_2")


EPSILON = 1e-06


def from_everyone(x, axis):
    count = lax.axis_size(axis)
    return lax.all_to_all(jnp.broadcast_to(x[None], (count, *x.shape)), axis, 0, 0, tiled=True)


def taken_together(x, axis):
    return from_everyone(x, axis).astype(jnp.float32).sum(axis=0)


def in_order(parts, dim):
    shape = list(parts.shape[1:])
    shape[dim] *= parts.shape[0]
    return jnp.moveaxis(parts, 0, dim).reshape(shape)


def whole_of(x, axes, dim):
    far, near = axes
    parts = from_everyone(from_everyone(x, far), near)
    return in_order(parts.swapaxes(0, 1).reshape(-1, *x.shape), dim)


def in_blocks(x, dim, count):
    shape = x.shape
    parts = x.reshape(*shape[:dim], count, shape[dim] // count, *shape[dim + 1 :])
    return jnp.moveaxis(parts, dim, 0)


def sent_and_summed(x, axis, dim):
    count = lax.axis_size(axis)
    parts = lax.all_to_all(in_blocks(x, dim, count), axis, 0, 0, tiled=True)
    return jnp.sum(parts.astype(jnp.float32), axis=0)


def sum_in_two_steps(x, axes, dim):
    far, near = axes
    parts = in_blocks(x, dim, lax.axis_size(far))
    nearer = sent_and_summed(parts, near, dim + 1)
    arrived = lax.all_to_all(
        nearer.astype(jnp.bfloat16), far, split_axis=0, concat_axis=0, tiled=True
    )
    return arrived.astype(jnp.float32).sum(axis=0)


def rms_scale(values, gain_row):
    mean_square = jnp.mean(values * values, axis=-1, keepdims=True)
    return values * lax.rsqrt(mean_square + EPSILON) * gain_row


def shards(
    tokens,
    attn_gain,
    w_query,
    w_key,
    w_value,
    w_forget,
    forget_bias,
    query_gain,
    key_gain,
    cache_pairs,
    cache_cum,
    lengths,
    w_output,
    ffn_gain,
    expert_ids,
    route_weight,
    w_exp_gate,
    w_exp_up,
    w_exp_down,
    shared_gate,
    w_dense_gate,
    w_dense_up,
    w_dense_down,
):
    seq_rows, width = tokens.shape
    head_size = query_gain.shape[0]
    kv_here = cache_pairs.shape[1]
    cache_len = cache_pairs.shape[2]
    tokens_f = tokens.astype(jnp.float32)
    normed = rms_scale(tokens_f, attn_gain).astype(jnp.bfloat16)
    query_raw = jnp.dot(normed, w_query, preferred_element_type=jnp.float32)
    heads_here = query_raw.shape[1] // head_size
    group_size = heads_here // kv_here
    query_rows = rms_scale(
        query_raw.reshape(seq_rows, kv_here, group_size, head_size), query_gain
    ).astype(jnp.bfloat16)
    key_raw = jnp.dot(normed, w_key, preferred_element_type=jnp.float32).reshape(
        seq_rows, kv_here, head_size
    )
    fresh_key = rms_scale(key_raw, key_gain).astype(jnp.bfloat16)
    value_new = jnp.dot(normed, w_value, preferred_element_type=jnp.float32).astype(jnp.bfloat16)
    value_new = value_new.reshape(seq_rows, kv_here, head_size)
    log_gate = jax.nn.log_sigmoid(
        jnp.dot(normed, w_forget, preferred_element_type=jnp.float32) + forget_bias
    )
    position = lax.broadcasted_iota(jnp.int32, (1, 1, cache_len), 2)
    is_live = position < lengths[:, None, None]
    last_cum = jnp.sum(jnp.where(position == lengths[:, None, None] - 1, cache_cum, 0.0), axis=2)
    now_cum = last_cum + log_gate
    cached_keys = cache_pairs[..., :head_size]
    cached_values = cache_pairs[..., head_size:]
    score_multiplier = head_size ** (-0.5)
    past_score = (
        jnp.einsum("bkgd,bkld->bkgl", query_rows, cached_keys, preferred_element_type=jnp.float32)
        * score_multiplier
    )
    past_score = past_score + (now_cum[:, :, None] - cache_cum)[:, :, None, :]
    past_score = jnp.where(is_live[:, :, None, :], past_score, -jnp.inf)
    current_score = (
        jnp.einsum("nlte,nle->nlt", query_rows, fresh_key, preferred_element_type=jnp.float32)
        * score_multiplier
    )
    row_peak = jnp.maximum(jnp.max(past_score, axis=3), current_score)
    past_exp = jnp.exp(past_score - row_peak[..., None])
    own_exp = jnp.exp(current_score - row_peak)
    denom_sum = jnp.sum(past_exp, axis=3) + own_exp
    past_prob = (past_exp / denom_sum[..., None]).astype(jnp.bfloat16)
    own_prob = (own_exp / denom_sum).astype(jnp.bfloat16)
    head_mix = jnp.einsum(
        "bkgl,bkld->bkgd", past_prob, cached_values, preferred_element_type=jnp.float32
    )
    head_mix = head_mix + own_prob[..., None].astype(jnp.float32) * value_new[:, :, None, :].astype(
        jnp.float32
    )
    head_mix = head_mix.astype(jnp.bfloat16).reshape(seq_rows, heads_here * head_size)
    partial_value = jnp.dot(head_mix, w_output, preferred_element_type=jnp.float32)
    attn_out = taken_together(partial_value.astype(jnp.bfloat16), "tp").astype(jnp.float32)
    residual = (tokens_f + attn_out).astype(jnp.bfloat16)
    residual_f = residual.astype(jnp.float32)
    normed_two = rms_scale(residual_f, ffn_gain).astype(jnp.bfloat16)
    all_rows = whole_of(normed_two, (("ep_0", "ep_1"), "ep_2"), 0)
    batch_rows = all_rows.shape[0]
    num_groups = lax.axis_size(EP)
    capacity = max(2, min(seq_rows, 128 // num_groups))
    chosen = expert_ids == lax.axis_index(EP)
    is_hit = jnp.sum(chosen.astype(jnp.int32), axis=1).reshape(num_groups, seq_rows)
    weight_here = jnp.sum(jnp.where(chosen, route_weight, 0.0), axis=1)
    slot_rank = jnp.cumsum(is_hit, axis=1)
    slot_ids = lax.broadcasted_iota(jnp.int32, (1, capacity, 1), 1) + 1
    picker = ((slot_rank[:, None, :] == slot_ids) & (is_hit[:, None, :] == 1)).astype(jnp.bfloat16)
    grouped = all_rows.reshape(num_groups, seq_rows, width)
    picked = jnp.einsum("scn,snd->scd", picker, grouped, preferred_element_type=jnp.float32)
    picked = picked.astype(jnp.bfloat16).reshape(num_groups * capacity, width)
    gate_part = jnp.dot(picked, w_exp_gate[0], preferred_element_type=jnp.float32)
    up_part = jnp.dot(picked, w_exp_up[0], preferred_element_type=jnp.float32)
    hidden = (jax.nn.silu(gate_part) * up_part).astype(jnp.bfloat16)
    expert_part = jnp.dot(hidden, w_exp_down[0], preferred_element_type=jnp.float32)
    expert_rows = sent_and_summed(expert_part.astype(jnp.bfloat16), "tp", 1).astype(jnp.bfloat16)
    feature_span = expert_rows.shape[1]
    placed = jnp.einsum(
        "scn,scd->snd",
        picker,
        expert_rows.reshape(num_groups, capacity, feature_span),
        preferred_element_type=jnp.float32,
    ).reshape(batch_rows, feature_span)
    expert_term = placed * weight_here[:, None]
    contract = (((1,), (1,)), ((), ()))
    dense_gate_raw = lax.dot_general(
        all_rows, w_dense_gate, contract, preferred_element_type=jnp.float32
    )
    dense_up_raw = lax.dot_general(
        all_rows, w_dense_up, contract, preferred_element_type=jnp.float32
    )
    dense_hidden = (jax.nn.silu(dense_gate_raw) * dense_up_raw).astype(jnp.bfloat16)
    mix_gate = jax.nn.sigmoid(jnp.dot(all_rows, shared_gate, preferred_element_type=jnp.float32))
    dense_rows = jnp.dot(dense_hidden, w_dense_down, preferred_element_type=jnp.float32)
    summed = sum_in_two_steps(
        (mix_gate[:, None] * dense_rows + expert_term).astype(jnp.bfloat16),
        (("ep_0", "ep_1"), "ep_2"),
        0,
    )
    column = lax.axis_index("tp") * feature_span
    own_residual = lax.dynamic_slice_in_dim(residual_f, column, feature_span, 1)
    return (own_residual + summed).astype(jnp.bfloat16)


def solution(mesh):
    split = Mesh(mesh.devices.reshape(8, 4, 2, mesh.shape["tp"]), ("ep_0", "ep_1", "ep_2", "tp"))
    return jax.shard_map(
        shards,
        mesh=split,
        in_specs=(
            P(EP, None),
            P(),
            P(None, "tp"),
            P(None, "tp"),
            P(None, "tp"),
            P(None, "tp"),
            P("tp"),
            P(),
            P(),
            P(EP, "tp", None, None),
            P(EP, "tp", None),
            P(EP),
            P("tp", None),
            P(),
            P(),
            P(),
            P(EP, None, "tp"),
            P(EP, None, "tp"),
            P(EP, "tp", None),
            P(),
            P(EP, None),
            P(EP, None),
            P(EP, "tp"),
        ),
        out_specs=P(EP, "tp"),
        check_vma=False,
    )
```

profile of v0, /device:TPU:1, one launch (start us, length us, event | category | flops | bytes accessed | tf_op | source)
XLA Modules:
  0.0 138.5 jit_solution(6740849996699019402)
XLA Ops:
  2.5 1.3 fusion.88
  4.1 1.3 multiply_reduce_fusion.1
  6.1 1.3 fusion.63
  7.3 1.0 fusion.78
  8.4 1.0 broadcast_subtract_fusion
  10.5 4.8 %fusion.89 = (f32[24,4]{1,0:T(8,128)S(1)}, f32[24,4,1024]{2,1,0:T(4,128)S(1)}) fusion(f32[24,1024]{1,0:T(8,128)S(1)} %bitcast.98, bf16[24,4,64]{2,1,0:T(4,128)(2,1)S(1)} %multiply_convert_fusion.1, bf16[24,1,1024,128]{3,2,1,0:T(8,128)(2,1)} %param.32, pred[24,1024]{1,0:T(8,128)(4,1)S(1)} %iota_compare_fusion), kind=kOutput, calls=%fused_computation.109 | convolution fusion | flops 12976032 | bytes 6820224 | tf_op jit(solution)/shard_map/bkgd,bkld->bkgl/dot_general | solution.py:115
  15.8 2.0 %fusion.35 = bf16[24,4,64]{2,1,0:T(4,128)(2,1)S(1)} fusion(bf16[24,1,1024,128]{3,2,1,0:T(8,128)(2,1)S(1)} %copy-done.13, f32[24,4,1024]{2,1,0:T(4,128)S(1)} %get-tuple-element.14, f32[24,4]{1,0:T(8,128)S(1)} %get-tuple-element.8, f32[24,4]{1,0:T(8,128)S(1)} %multiply_maximum_fusion, f32[24,64]{1,0:T(8,128)S(1)} %fusion.41, f32[24,4]{1,0:T(8,128)S(1)} %get-tuple-element.7), kind=kOutput, calls=%fused_computation.26 | convolution fusion | flops 12896256 | bytes 6704256 | tf_op jit(solution)/shard_map/bkgl,bkld->bkgd/dot_general | solution.py:130
  18.1 9.8 %all_to_all.30 = bf16[4,24,1024]{2,1,0:T(8,128)(2,1)S(1)} all-to-all(bf16[4,24,1024]{2,1,0:T(8,128)(2,1)S(1)} %broadcast_in_dim.28), channel_id=1, replica_groups=mesh['ep_0'=8,'ep_1'=4,'ep_2'=2,'tp'=4] {'tp'}, dimensions={0} | all-to-all | bytes 393216 | tf_op jit(solution)/shard_map/all_to_all | solution.py:15
  28.2 1.3 broadcast_in_dim.29
  29.6 11.3 %all-to-all-start.1 = ((bf16[32,24,1024]{2,1,0:T(8,128)(2,1)}), bf16[32,24,1024]{2,1,0:T(8,128)(2,1)S(1)}, u32[]{:S(2)}, u32[]{:S(2)}) async-start(bf16[32,24,1024]{2,1,0:T(8,128)(2,1)} %broadcast_in_dim.29), calls=%async_computation.1 | async-start | bytes 3145728 | tf_op jit(solution)/shard_map/all_to_all | solution.py:15
  43.1 1.3 select_reduce_fusion
  45.2 31.5 %all-to-all-done.1 = bf16[32,24,1024]{2,1,0:T(8,128)(2,1)S(1)} async-done(((bf16[32,24,1024]{2,1,0:T(8,128)(2,1)}), bf16[32,24,1024]{2,1,0:T(8,128)(2,1)S(1)}, u32[]{:S(2)}, u32[]{:S(2)}) %all-to-all-start.1) | async-done | bytes 1572896 | tf_op jit(solution)/shard_map/all_to_all | solution.py:15
  77.2 10.1 %all_to_all.31 = bf16[2,32,24,1024]{3,2,1,0:T(8,128)(2,1)S(1)} all-to-all(bf16[2,32,24,1024]{3,2,1,0:T(8,128)(2,1)S(1)} %broadcast_in_dim.30), channel_id=1, replica_groups=mesh['ep_0'=8,'ep_1'=4,'ep_2'=2,'tp'=4] {'ep_2'}, dimensions={0} | all-to-all | bytes 6291456 | tf_op jit(solution)/shard_map/all_to_all | solution.py:15
  87.8 1.7 %copy-done.1 = bf16[2,32,24,1024]{3,2,0,1:T(8,128)(2,1)} copy-done((bf16[2,32,24,1024]{3,2,0,1:T(8,128)(2,1)}, bf16[2,32,24,1024]{3,2,0,1:T(8,128)(2,1)S(1)}, u32[]{:S(2)}) %copy-start.1) | copy-done | bytes 3145752
  90.4 1.9 %fusion.13 = f32[128,896]{1,0:T(8,128)S(1)} fusion(bf16[128,1024]{1,0:T(8,128)(2,1)S(1)} %reshape.261, bf16[1,1024,896]{2,1,0:T(8,128)(2,1)} %param.39), kind=kOutput, calls=%fused_computation.15 | convolution fusion | flops 234881024 | bytes 2555904 | tf_op jit(solution)/shard_map/dot_general | solution.py:155
  92.3 2.3 %fusion.18 = bf16[128,1024]{1,0:T(8,128)(2,1)S(1)} fusion(bf16[1,896,1024]{2,1,0:T(8,128)(2,1)S(1)} %copy-done, bf16[128,1024]{1,0:T(8,128)(2,1)S(1)} %reshape.261, bf16[1,1024,896]{2,1,0:T(8,128)(2,1)} %param.40, f32[128,896]{1,0:T(8,128)S(1)} %fusion.13), kind=kOutput, calls=%fused_computation.19 | convolution fusion | flops 470581248 | bytes 4653056 | tf_op jit(solution)/shard_map/dot_general | solution.py:158
  95.4 3.4 %all-to-all-start.3 = ((bf16[4,128,256]{2,1,0:T(8,128)(2,1)}), bf16[4,128,256]{2,1,0:T(8,128)(2,1)S(1)}, u32[]{:S(2)}, u32[]{:S(2)}) async-start(bf16[4,128,256]{2,1,0:T(8,128)(2,1)} %bitcast.88), calls=%async_computation.3 | async-start | bytes 524288 | tf_op jit(solution)/shard_map/all_to_all | solution.py:42
  98.8 3.9 %fusion.90 = f32[1536,64]{0,1:T(8,128)} fusion(bf16[1536,1024]{1,0:T(8,128)(2,1)} %bitcast.92, bf16[64,1024]{1,0:T(8,128)(2,1)S(1)} %copy-done.5), kind=kOutput, calls=%fused_computation.110 | convolution fusion | flops 201326592 | bytes 3670016 | tf_op jit(solution)/shard_map/dot_general | solution.py:169
  103.7 1.2 all-to-all-done.3
  106.5 4.3 %fusion.7 = bf16[1536,256]{1,0:T(8,128)(2,1)} fusion(f32[1536,256]{1,0:T(8,128)S(1)} %bitcast_multiply_fusion, bf16[64,256]{1,0:T(8,128)(2,1)S(1)} %copy-done.7, bf16[1536,1024]{1,0:T(8,128)(2,1)} %bitcast.93, bf16[64,1024]{1,0:T(8,128)(2,1)} %param.44, f32[1536]{0:T(1024)S(1)} %add_divide_fusion, f32[1536,64]{0,1:T(8,128)} %fusion.90), kind=kOutput, calls=%fused_computation.8 | convolution fusion | flops 253427712 | bytes 6068224 | tf_op jit(solution)/shard_map/dot_general | solution.py:177
  110.8 1.2 copy.54
  112.0 5.5 %all_to_all.32 = bf16[2,32,24,256]{3,2,1,0:T(8,128)(2,1)S(1)} all-to-all(bf16[2,32,24,256]{3,2,1,0:T(8,128)(2,1)S(1)} %bitcast.95), channel_id=1, replica_groups=mesh['ep_0'=8,'ep_1'=4,'ep_2'=2,'tp'=4] {'ep_2'}, dimensions={0} | all-to-all | bytes 1572864 | tf_op jit(solution)/shard_map/all_to_all | solution.py:42
  118.5 5.5 %all-to-all-start.5 = ((bf16[32,24,256]{2,1,0:T(8,128)(2,1)}), bf16[32,24,256]{2,1,0:T(8,128)(2,1)S(1)}, u32[]{:S(2)}, u32[]{:S(2)}) async-start(bf16[32,24,256]{2,1,0:T(8,128)(2,1)} %reduce_sum.124), calls=%async_computation.5 | async-start | bytes 786432 | tf_op jit(solution)/shard_map/all_to_all | solution.py:50
  124.0 13.9 %all-to-all-done.5 = bf16[32,24,256]{2,1,0:T(8,128)(2,1)S(1)} async-done(((bf16[32,24,256]{2,1,0:T(8,128)(2,1)}), bf16[32,24,256]{2,1,0:T(8,128)(2,1)S(1)}, u32[]{:S(2)}, u32[]{:S(2)}) %all-to-all-start.5) | async-done | bytes 393248 | tf_op jit(solution)/shard_map/all_to_all | solution.py:50
  (73 shorter events, 14.4 us)
Async XLA Ops:
  0.0 92.3 %copy-start = (bf16[1,896,1024]{2,1,0:T(8,128)(2,1)S(1)}, bf16[1,896,1024]{2,1,0:T(8,128)(2,1)}, u32[]{:S(2)}) copy-start(bf16[1,896,1024]{2,1,0:T(8,128)(2,1)} %param.41) | copy-start | bytes 5505028
  0.0 10.2 %copy-start.12 = (f32[64]{0:T(128)S(1)}, f32[64]{0:T(128)}, u32[]{:S(2)}) copy-start(f32[64]{0:T(128)} %param.31) | copy-start | bytes 772
  10.4 5.1 %copy-start.4 = (bf16[24,1024]{1,0:T(8,128)(2,1)S(1)}, bf16[24,1024]{1,0:T(8,128)(2,1)}, u32[]{:S(2)}) copy-start(bf16[24,1024]{1,0:T(8,128)(2,1)} %param.23) | copy-start | bytes 147460
  10.4 5.1 %copy-start.8 = (f32[1024]{0:T(1024)S(1)}, f32[1024]{0:T(1024)}, u32[]{:S(2)}) copy-start(f32[1024]{0:T(1024)} %param.24) | copy-start | bytes 12292
  10.4 5.1 %copy-start.14 = (bf16[1024,64]{0,1:T(8,128)(2,1)S(1)}, bf16[1024,64]{0,1:T(8,128)(2,1)}, u32[]{:S(2)}) copy-start(bf16[1024,64]{0,1:T(8,128)(2,1)} %param.27) | copy-start | bytes 393220
  10.5 5.3 %copy-start.13 = (bf16[24,1,1024,128]{3,2,1,0:T(8,128)(2,1)S(1)}, bf16[24,1,1024,128]{3,2,1,0:T(8,128)(2,1)}, u32[]{:S(2)}) copy-start(bf16[24,1,1024,128]{3,2,1,0:T(8,128)(2,1)} %param.32) | copy-start | bytes 18874372
  15.8 2.1 %copy-start.3 = (bf16[256,1024]{1,0:T(8,128)(2,1)S(1)}, bf16[256,1024]{1,0:T(8,128)(2,1)}, u32[]{:S(2)}) copy-start(bf16[256,1024]{1,0:T(8,128)(2,1)} %param.35) | copy-start | bytes 1572868
  15.8 12.3 %copy-start.9 = (f32[1024]{0:T(1024)S(1)}, f32[1024]{0:T(1024)}, u32[]{:S(2)}) copy-start(f32[1024]{0:T(1024)} %param.36) | copy-start | bytes 12292
  29.6 11.4 %copy-start.6 = (s32[1536,2]{0,1:T(2,128)S(1)}, s32[1536,2]{0,1:T(2,128)}, u32[]{:S(2)}) copy-start(s32[1536,2]{0,1:T(2,128)} %param.37) | copy-start | bytes 36868
  29.6 12.1 %copy-start.11 = (bf16[1024]{0:T(1024)(128)(2,1)S(1)}, bf16[1024]{0:T(1024)(128)(2,1)}, u32[]{:S(2)}) copy-start(bf16[1024]{0:T(1024)(128)(2,1)} %param.42) | copy-start | bytes 6148
  29.6 47.1 %all-to-all-start.1 = ((bf16[32,24,1024]{2,1,0:T(8,128)(2,1)}), bf16[32,24,1024]{2,1,0:T(8,128)(2,1)S(1)}, u32[]{:S(2)}, u32[]{:S(2)}) async-start(bf16[32,24,1024]{2,1,0:T(8,128)(2,1)} %broadcast_in_dim.29), calls=%async_computation.1 | async-start | bytes 3145728 | tf_op jit(solution)/shard_map/all_to_all | solution.py:15
  87.3 2.1 %copy-start.10 = (s32[2]{0:T(128)S(1)}, s32[2]{0:T(128)}, u32[]{:S(2)}) copy-start(s32[2]{0:T(128)} %iota_add_fusion) | copy-start | bytes 28
  87.8 1.7 %copy-start.1 = (bf16[2,32,24,1024]{3,2,0,1:T(8,128)(2,1)}, bf16[2,32,24,1024]{3,2,0,1:T(8,128)(2,1)S(1)}, u32[]{:S(2)}) copy-start(bf16[2,32,24,1024]{3,2,0,1:T(8,128)(2,1)S(1)} %copy.40) | copy-start | bytes 9437188
  92.3 6.5 %copy-start.5 = (bf16[64,1024]{1,0:T(8,128)(2,1)S(1)}, bf16[64,1024]{1,0:T(8,128)(2,1)}, u32[]{:S(2)}) copy-start(bf16[64,1024]{1,0:T(8,128)(2,1)} %param.43) | copy-start | bytes 393220
  95.4 9.5 %all-to-all-start.3 = ((bf16[4,128,256]{2,1,0:T(8,128)(2,1)}), bf16[4,128,256]{2,1,0:T(8,128)(2,1)S(1)}, u32[]{:S(2)}, u32[]{:S(2)}) async-start(bf16[4,128,256]{2,1,0:T(8,128)(2,1)} %bitcast.88), calls=%async_computation.3 | async-start | bytes 524288 | tf_op jit(solution)/shard_map/all_to_all | solution.py:42
  98.8 3.9 %copy-start.2 = (bf16[2,32,24,1024]{3,2,0,1:T(8,128)(2,1)S(1)}, bf16[2,32,24,1024]{3,2,0,1:T(8,128)(2,1)}, u32[]{:S(2)}) copy-start(bf16[2,32,24,1024]{3,2,0,1:T(8,128)(2,1)} %copy-done.1) | copy-start | bytes 9437188
  105.5 1.0 copy-start.7
  118.5 19.4 %all-to-all-start.5 = ((bf16[32,24,256]{2,1,0:T(8,128)(2,1)}), bf16[32,24,256]{2,1,0:T(8,128)(2,1)S(1)}, u32[]{:S(2)}, u32[]{:S(2)}) async-start(bf16[32,24,256]{2,1,0:T(8,128)(2,1)} %reduce_sum.124), calls=%async_computation.5 | async-start | bytes 786432 | tf_op jit(solution)/shard_map/all_to_all | solution.py:50
where the time goes:
time: 140 us; the launch traced here: 139 us
  waiting for transfers between devices  46.6 us (33%)
  matrix products  25.6 us (18%)
  blocking collectives  25.5 us (18%)
  starting transfers between devices  20.2 us (14%)
  other arithmetic  12.5 us (9%)
  local copies, waits for them, and re-layouts  7.02 us (5%)
    all_to_all x1, waiting for transfers between devices, from_everyone(): lax.all_to_all(jnp.broadcast_to(x[None], (count, *x.shape)), axis, 0, 0,...  31.5 us
    all_to_all x2, blocking collectives, from_everyone(): lax.all_to_all(jnp.broadcast_to(x[None], (count, *x.shape)), axis, 0, 0,...  20 us
    all_to_all x1, waiting for transfers between devices, sum_in_two_steps(): lax.all_to_all(nearer.astype(jnp.bfloat16), far, split_axis=0, concat_axi...  13.9 us
    all_to_all x1, starting transfers between devices, from_everyone(): lax.all_to_all(jnp.broadcast_to(x[None], (count, *x.shape)), axis, 0, 0,...  11.3 us
    all_to_all x1, blocking collectives, sent_and_summed(): parts = lax.all_to_all(in_blocks(x, dim, count), axis, 0, 0, tiled=True)  5.52 us
    all_to_all x1, starting transfers between devices, sum_in_two_steps(): lax.all_to_all(nearer.astype(jnp.bfloat16), far, split_axis=0, concat_axi...  5.48 us
    dot_general x1, matrix products, shards(): jnp.einsum('bkgd,bkld->bkgl', query_rows, cached_keys, preferred_element_...  4.76 us
    dot_general x1, matrix products, shards(): jnp.dot(dense_hidden, w_dense_down, preferred_element_type=jnp.float32)  4.33 us
  transfers between devices with their start and end apart: 3, of which 3 were waited for; matrix products, arithmetic and copies ran while one was open for 7% of the time, Pallas kernels for 0%

commit v1 on v0

v1 whole, which is shorter than its diff:
```python
import functools

import jax
import jax.numpy as jnp
from jax import lax
from jax.experimental import pallas as pl
from jax.experimental.pallas import tpu as pltpu
from jax.sharding import PartitionSpec as P

EPSILON = 1e-06
MESH = pl.DeviceIdType.MESH
BF = jnp.bfloat16
F32 = jnp.float32
GROUP = 8
NEG = -1e30


def iota(shape, dim):
    return lax.broadcasted_iota(jnp.int32, shape, dim)


def dot(a, b):
    return jnp.dot(a, b, preferred_element_type=F32)


def dot_nt(a, b):
    return lax.dot_general(a, b, (((1,), (1,)), ((), ())), preferred_element_type=F32)


def rms(values):
    return lax.rsqrt(jnp.mean(values * values, axis=-1, keepdims=True) + EPSILON)


def silu(v):
    return v / (1.0 + jnp.exp(-v))


def one_hot(cond):
    return jnp.where(cond, 1.0, 0.0).astype(BF)


def kernel(
    n_ep,
    n_tp,
    tokens_h,
    attn_gain_h,
    w_query_h,
    w_key_h,
    w_value_h,
    w_forget_h,
    forget_bias_h,
    query_gain_h,
    key_gain_h,
    cache_h,
    cum_h,
    lengths_h,
    w_output_h,
    ffn_gain_h,
    ids_h,
    route_h,
    w_gate_h,
    w_up_h,
    w_down_h,
    shared_gate_h,
    dense_gate_h,
    dense_up_h,
    dense_down_h,
    out_ref,
    tok,
    again,
    wq,
    wk,
    wv,
    wf,
    fb,
    qg,
    kg,
    cache,
    cum,
    lens,
    wo,
    fgain,
    ids,
    route,
    wg,
    wu,
    wd,
    sg,
    gz,
    uz,
    dz,
    bias_rows,
    q_rows,
    mix_rows,
    xr,
    resid,
    dt,
    send_rows,
    recv_rows,
    hx,
    dsend,
    drecv,
    esend,
    erecv,
    back_send,
    back_recv,
    comb_hi,
    comb_lo,
    pick,
    load_sem,
    cache_sem,
    weight_sem,
    z_local_sem,
    z_send,
    z_recv,
    x_send,
    x_recv,
    a_send,
    a_recv,
    t_send,
    t_recv,
    h_send,
    h_recv,
    d_send,
    d_recv,
    e_send,
    e_recv,
    b_send,
    b_recv,
):
    ep = lax.axis_index("ep")
    tp = lax.axis_index("tp")
    rows, width = tok.shape
    n_z = n_ep // GROUP
    g = lax.rem(ep, GROUP)
    base = ep - g
    head = qg.shape[1]
    span = width // n_tp
    units = gz.shape[1]

    def x_peer(k):
        return {"ep": ep, "tp": lax.rem(tp + k, n_tp)}

    def group_peer(k):
        return {"ep": base + lax.rem(g + k, GROUP), "tp": tp}

    def z_peer(k):
        return {"ep": lax.rem(ep + GROUP * k, n_ep), "tp": tp}

    small = [
        (tokens_h, tok),
        (attn_gain_h, again),
        (w_query_h, wq),
        (w_key_h, wk),
        (w_value_h, wv),
        (w_forget_h, wf),
        (forget_bias_h, fb),
        (query_gain_h, qg),
        (key_gain_h, kg),
        (cum_h, cum),
        (lengths_h, lens),
    ]
    loads = [pltpu.make_async_copy(s, d, load_sem.at[i]) for i, (s, d) in enumerate(small)]
    for c in loads:
        c.start()
    barrier = pltpu.get_barrier_semaphore()

    def greet(k, carry):
        pl.semaphore_signal(
            barrier,
            inc=1,
            device_id={"ep": lax.rem(ep + k, n_ep), "tp": tp},
            device_id_type=MESH,
        )
        return carry

    lax.fori_loop(1, n_ep, greet, 0)
    for k in range(1, n_tp):
        pl.semaphore_signal(barrier, inc=1, device_id=x_peer(k), device_id_type=MESH)
    cache_loads = []
    for s in range(rows):
        c = pltpu.make_async_copy(
            cache_h.at[s, 0], cache.at[s // 2, :, pl.ds(128 * (s % 2), 128)], cache_sem.at[s]
        )
        c.start()
        cache_loads.append(c)
    later = [
        (w_output_h, wo),
        (ffn_gain_h, fgain),
        (ids_h, ids),
        (route_h, route),
        (shared_gate_h, sg),
        (w_gate_h.at[0], wg),
        (w_up_h.at[0], wu),
        (w_down_h.at[0], wd),
    ]
    late_loads = [pltpu.make_async_copy(s, d, weight_sem.at[i]) for i, (s, d) in enumerate(later)]
    for c in late_loads:
        c.start()
    quarter = pl.ds(pl.multiple_of(tp * units, units), units)
    own_dense = [
        pltpu.make_async_copy(dense_gate_h.at[quarter], gz.at[0], z_local_sem.at[0]),
        pltpu.make_async_copy(dense_up_h.at[quarter], uz.at[0], z_local_sem.at[1]),
        pltpu.make_async_copy(dense_down_h, dz.at[0], z_local_sem.at[2]),
    ]
    for c in own_dense:
        c.start()

    for c in loads:
        c.wait()
    tokens_f = tok[...].astype(F32)
    normed = (tokens_f * rms(tokens_f) * again[...]).astype(BF)
    query_raw = dot(normed, wq[...])
    key_raw = dot_nt(normed, wk[...])
    value_new = dot_nt(normed, wv[...]).astype(BF)
    forget = jnp.sum(normed.astype(F32) * wf[...].astype(F32), axis=1, keepdims=True)
    forget = forget + fb[...]
    log_gate = jnp.minimum(forget, 0.0) - jnp.log1p(jnp.exp(-jnp.abs(forget)))

    lane_q = iota((rows, span), 1)
    squares = query_raw * query_raw
    scale = jnp.zeros((rows, span), F32)
    for h in range(span // head):
        here = lane_q // head == h
        total = jnp.sum(jnp.where(here, squares, 0.0), axis=1, keepdims=True)
        scale = jnp.where(here, lax.rsqrt(total / head + EPSILON), scale)
    gains = jnp.concatenate([qg[...]] * (span // head), axis=1)
    queries = (query_raw * scale * gains).astype(BF).astype(F32) * head ** (-0.5)
    queries = queries.astype(BF)
    key_new = (key_raw * rms(key_raw) * kg[...]).astype(BF)

    heads = span // head
    n_rows = rows * heads
    row_r = iota((n_rows, 256), 0)
    lane_r = iota((n_rows, 256), 1)
    seq_of = one_hot(iota((n_rows, rows), 0) // heads == iota((n_rows, rows), 1))
    own_half = lane_r // 128 == (row_r // heads) % 2
    own_head = lane_r // head == row_r % heads
    low = own_half & (lane_r % 128 < head)
    high = own_half & (lane_r % 128 >= head)
    fold = one_hot(iota((256, 256), 0) % head == iota((256, 256), 1) % head)
    spread = one_hot(iota((head, 256), 0) == iota((head, 256), 1) % head)

    q_all = jnp.where(own_head, dot(seq_of, queries), 0.0).astype(BF)
    q_wide = jnp.where(low, dot(q_all, fold), 0.0)
    q_rows[...] = q_wide
    key_wide = dot(seq_of, dot(key_new, spread).astype(BF))
    own_score = jnp.sum(q_wide * key_wide, axis=1, keepdims=True)
    value_wide = jnp.where(high, dot(seq_of, dot(value_new, spread).astype(BF)), 0.0)

    cum_2d = cum[...].reshape(rows, cum.shape[2])
    slots = cum_2d.shape[1]
    lens_f = lens[...].astype(F32)
    lens_col = jnp.sum(
        jnp.where(iota((rows, rows), 0) == iota((rows, rows), 1), lens_f, 0.0),
        axis=1,
        keepdims=True,
    )
    position = iota((rows, slots), 1).astype(F32)
    last_cum = jnp.sum(jnp.where(position == lens_col - 1.0, cum_2d, 0.0), axis=1, keepdims=True)
    now_cum = last_cum + log_gate
    bias_rows[...] = jnp.where(position < lens_col, now_cum - cum_2d, NEG)

    pl.semaphore_wait(barrier, n_ep - 1 + n_tp - 1)
    z_copies = []
    for k in (4, 3, 5, 2, 6, 1, 7):
        for i, (src, dst) in enumerate(
            ((dense_gate_h.at[quarter], gz), (dense_up_h.at[quarter], uz), (dense_down_h, dz))
        ):
            z_copies.append(
                pltpu.make_async_remote_copy(
                    src_ref=src,
                    dst_ref=dst.at[k],
                    send_sem=z_send.at[i, k],
                    recv_sem=z_recv.at[i, k],
                    device_id=z_peer(k),
                    device_id_type=MESH,
                )
            )
    for c in z_copies:
        c.start()

    pair = 2 * heads
    first = iota((pair, slots), 0) < heads
    own_probs = []
    for p in range(rows // 2):
        cache_loads[2 * p].wait()
        cache_loads[2 * p + 1].wait()
        q_pair = q_rows[pl.ds(pair * p, pair), :].astype(BF)
        score = jnp.concatenate(
            [dot_nt(q_pair, cache[p, pl.ds(256 * c, 256), :]) for c in range(slots // 256)], axis=1
        )
        decay = jnp.where(
            first,
            jnp.broadcast_to(bias_rows[pl.ds(2 * p, 1), :], (pair, slots)),
            jnp.broadcast_to(bias_rows[pl.ds(2 * p + 1, 1), :], (pair, slots)),
        )
        score = score + decay
        own = own_score[pair * p : pair * (p + 1)]
        peak = jnp.maximum(jnp.max(score, axis=1, keepdims=True), own)
        past = jnp.exp(score - peak)
        own_exp = jnp.exp(own - peak)
        inverse = 1.0 / (jnp.sum(past, axis=1, keepdims=True) + own_exp)
        prob = (past * inverse).astype(BF)
        own_probs.append((own_exp * inverse).astype(BF).astype(F32))
        mix_rows[pl.ds(pair * p, pair), :] = dot(prob, cache[p])
    mixed = jnp.where(high, mix_rows[...], 0.0)
    mixed = mixed + jnp.concatenate(own_probs, axis=0) * value_wide
    by_head = jnp.where(own_head, dot(mixed.astype(BF), fold), 0.0).astype(BF)
    to_seq = one_hot(iota((rows, n_rows), 1) // heads == iota((rows, n_rows), 0))
    head_mix = dot(to_seq, by_head).astype(BF)
    for c in late_loads[:5]:
        c.wait()
    xr[0] = dot(head_mix, wo[...]).astype(BF)
    x_copies = []
    for k in (2, 1, 3):
        c = pltpu.make_async_remote_copy(
            src_ref=xr.at[0],
            dst_ref=xr.at[k],
            send_sem=x_send.at[k],
            recv_sem=x_recv.at[k],
            device_id=x_peer(k),
            device_id_type=MESH,
        )
        c.start()
        x_copies.append(c)

    n_pick = 2 * n_ep
    tokens_all = ids.shape[1]
    window = 256
    first_lane = ep * rows
    start = jnp.minimum(first_lane // 128, (tokens_all - window) // 128) * 128
    offset = first_lane - start
    pick_lanes = iota((window, 128), 0) == iota((window, 128), 1) + offset
    pick_lanes = jnp.where(pick_lanes & (iota((window, 128), 1) < rows), 1.0, 0.0)
    lanes = pl.ds(pl.multiple_of(start, 128), window)
    both = jnp.concatenate([ids[:, lanes].astype(F32), route[:, lanes]], axis=0)
    mine = jnp.dot(both, pick_lanes, precision=lax.Precision.HIGHEST, preferred_element_type=F32)
    lane_p = iota((n_pick, 128), 1)
    expert = (iota((n_pick, 128), 0) // 2).astype(F32)
    live = lane_p < rows
    hit_0 = (mine[0:1] == expert) & live
    hit_1 = (mine[1:2] == expert) & live
    hit = one_hot(hit_0 | hit_1)
    rank = dot(hit, one_hot(iota((128, 128), 0) <= iota((128, 128), 1)))
    slot = (iota((n_pick, 128), 0) % 2 + 1).astype(F32)
    picked = jnp.where((rank == slot) & (hit.astype(F32) > 0.5), 1.0, 0.0)
    pick[...] = picked.astype(BF)
    weight = jnp.where(hit_0, mine[2:3], 0.0) + jnp.where(hit_1, mine[3:4], 0.0)
    combine = (picked * weight).T
    combine_hi = combine.astype(BF)
    comb_hi[...] = combine_hi
    comb_lo[...] = (combine - combine_hi.astype(F32)).astype(BF)

    for c in x_copies:
        c.wait_recv()
    attn_out = xr[0].astype(F32) + xr[1].astype(F32) + xr[2].astype(F32) + xr[3].astype(F32)
    residual = (tok[...].astype(F32) + attn_out).astype(BF).astype(F32)
    resid[...] = residual
    normed_two = (residual * rms(residual) * fgain[...]).astype(BF)
    dt[0] = normed_two
    mix_gate = jnp.sum(normed_two.astype(F32) * sg[...].astype(F32), axis=1, keepdims=True)
    mix_gate = 1.0 / (1.0 + jnp.exp(-mix_gate))
    packed = dot(pick[:, :rows], normed_two).astype(BF)
    send_rows[...] = packed.reshape(n_ep, 2, width)
    recv_rows[ep] = send_rows[ep]

    def dispatch(k, carry):
        to = lax.rem(ep + k, n_ep)
        pltpu.make_async_remote_copy(
            src_ref=send_rows.at[to],
            dst_ref=recv_rows.at[ep],
            send_sem=a_send,
            recv_sem=a_recv,
            device_id={"ep": to, "tp": tp},
            device_id_type=MESH,
        ).start()
        return carry

    lax.fori_loop(1, n_ep, dispatch, 0)
    t_copies = []
    for k in range(1, GROUP):
        c = pltpu.make_async_remote_copy(
            src_ref=dt.at[0],
            dst_ref=dt.at[k],
            send_sem=t_send.at[k],
            recv_sem=t_recv.at[k],
            device_id=group_peer(k),
            device_id_type=MESH,
        )
        c.start()
        t_copies.append(c)

    for c in late_loads[5:]:
        c.wait()
    others = pl.ds(0, n_ep - 1)
    arrivals = pltpu.make_async_remote_copy(
        src_ref=send_rows.at[others],
        dst_ref=recv_rows.at[others],
        send_sem=a_send,
        recv_sem=a_recv,
        device_id=x_peer(1),
        device_id_type=MESH,
    )
    arrivals.wait_recv()
    routed = recv_rows[...].reshape(n_pick, width)
    hidden = (silu(dot(routed, wg[...])) * dot(routed, wu[...])).astype(BF)
    e_copies = []
    for k in (2, 1, 3, 0):
        column = pl.ds(pl.multiple_of(lax.rem(tp + k, n_tp) * span, span), span)
        esend[k] = dot(hidden, wd[:, column]).astype(BF)
        if k:
            c = pltpu.make_async_remote_copy(
                src_ref=esend.at[k],
                dst_ref=erecv.at[k],
                send_sem=e_send.at[k],
                recv_sem=e_recv.at[k],
                device_id=x_peer(k),
                device_id_type=MESH,
            )
            c.start()
            e_copies.append(c)

    for c in own_dense:
        c.wait()
    for c in z_copies:
        c.wait_recv()
    for c in t_copies:
        c.wait_recv()
    group_rows = dt[...].reshape(GROUP * rows, width)
    dense_w = n_z * units
    dense_gate = dot_nt(group_rows, gz[...].reshape(dense_w, width))
    dense_up = dot_nt(group_rows, uz[...].reshape(dense_w, width))
    hx[0] = (silu(dense_gate) * dense_up).astype(BF)
    h_copies = []
    for k in (2, 1, 3):
        c = pltpu.make_async_remote_copy(
            src_ref=hx.at[0],
            dst_ref=hx.at[k],
            send_sem=h_send.at[k],
            recv_sem=h_recv.at[k],
            device_id=x_peer(k),
            device_id_type=MESH,
        )
        c.start()
        h_copies.append(c)

    for c in e_copies:
        c.wait_recv()
    summed = esend[0].astype(F32) + erecv[1].astype(F32) + erecv[2].astype(F32)
    summed = (summed + erecv[3].astype(F32)).astype(BF)
    back_send[...] = summed.reshape(n_ep, 2, span)
    back_recv[ep] = back_send[ep]

    def give_back(k, carry):
        to = lax.rem(ep + k, n_ep)
        pltpu.make_async_remote_copy(
            src_ref=back_send.at[to],
            dst_ref=back_recv.at[ep],
            send_sem=b_send,
            recv_sem=b_recv,
            device_id={"ep": to, "tp": tp},
            device_id_type=MESH,
        ).start()
        return carry

    lax.fori_loop(1, n_ep, give_back, 0)

    for c in h_copies:
        c.wait_recv()
    dense_part = jnp.zeros((GROUP * rows, span), F32)
    for k in range(n_tp):
        owner = lax.rem(tp + n_tp - k, n_tp)
        part = dz[:, pl.ds(pl.multiple_of(owner * units, units), units), :]
        dense_part = dense_part + dot(hx[k], part.reshape(dense_w, span))
    dsend[...] = dense_part.astype(BF).reshape(GROUP, rows, span)
    d_copies = []
    for k in range(1, GROUP):
        c = pltpu.make_async_remote_copy(
            src_ref=dsend.at[k],
            dst_ref=drecv.at[k],
            send_sem=d_send.at[k],
            recv_sem=d_recv.at[k],
            device_id=group_peer(GROUP - k),
            device_id_type=MESH,
        )
        c.start()
        d_copies.append(c)
    for c in d_copies:
        c.wait_recv()
    dense_sum = dsend[0].astype(F32)
    for k in range(1, GROUP):
        dense_sum = dense_sum + drecv[k].astype(F32)

    returned = pltpu.make_async_remote_copy(
        src_ref=back_send.at[others],
        dst_ref=back_recv.at[others],
        send_sem=b_send,
        recv_sem=b_recv,
        device_id=x_peer(1),
        device_id_type=MESH,
    )
    returned.wait_recv()
    expert_rows = back_recv[...].reshape(n_pick, span)
    expert_sum = dot(comb_hi[...], expert_rows) + dot(comb_lo[...], expert_rows)
    mine_cols = pl.ds(pl.multiple_of(tp * span, span), span)
    out = resid[:, mine_cols] + expert_sum[:rows] + mix_gate * dense_sum
    out_ref[...] = out.astype(BF)

    for c in z_copies + x_copies + t_copies + e_copies + h_copies + d_copies:
        c.wait_send()
    arrivals.wait_send()
    returned.wait_send()


def solution(mesh):
    n_ep, n_tp = mesh.shape["ep"], mesh.shape["tp"]

    def shards(*args):
        (
            tokens,
            attn_gain,
            w_query,
            w_key,
            w_value,
            w_forget,
            forget_bias,
            query_gain,
            key_gain,
            cache_pairs,
            cache_cum,
            lengths,
            w_output,
            ffn_gain,
            expert_ids,
            route_weight,
            w_exp_gate,
            w_exp_up,
            w_exp_down,
            shared_gate,
            w_dense_gate,
            w_dense_up,
            w_dense_down,
        ) = args
        rows, width = tokens.shape
        head = query_gain.shape[0]
        slots = cache_pairs.shape[2]
        span = width // n_tp
        n_rows = rows * (w_query.shape[1] // head)
        units = w_dense_gate.shape[0] // n_tp
        n_z = n_ep // GROUP
        ff = w_exp_gate.shape[2]
        n_pick = 2 * n_ep
        operands = (
            tokens,
            attn_gain.reshape(1, -1),
            w_query,
            w_key.T,
            w_value.T,
            w_forget.T,
            forget_bias.reshape(1, -1),
            query_gain.reshape(1, -1),
            key_gain.reshape(1, -1),
            cache_pairs,
            cache_cum,
            lengths.reshape(1, -1),
            w_output,
            ffn_gain.reshape(1, -1),
            expert_ids.T,
            route_weight.T,
            w_exp_gate,
            w_exp_up,
            w_exp_down,
            shared_gate.reshape(1, -1),
            w_dense_gate,
            w_dense_up,
            w_dense_down,
        )
        dma = pltpu.SemaphoreType.DMA
        vmem = pltpu.VMEM
        like = lambda a: vmem(a.shape, a.dtype)
        scratch = [
            like(tokens),
            like(operands[1]),
            like(w_query),
            like(operands[3]),
            like(operands[4]),
            like(operands[5]),
            like(operands[6]),
            like(operands[7]),
            like(operands[8]),
            vmem((rows // 2, slots, 256), BF),
            like(cache_cum),
            like(operands[11]),
            like(w_output),
            like(operands[13]),
            like(operands[14]),
            like(operands[15]),
            vmem((width, ff), BF),
            vmem((width, ff), BF),
            vmem((ff, width), BF),
            like(operands[19]),
            vmem((n_z, units, width), BF),
            vmem((n_z, units, width), BF),
            vmem((n_z, units * n_tp, span), BF),
            vmem((rows, slots), F32),
            vmem((n_rows, 256), F32),
            vmem((n_rows, 256), F32),
            vmem((n_tp, rows, width), BF),
            vmem((rows, width), F32),
            vmem((GROUP, rows, width), BF),
            vmem((n_ep, 2, width), BF),
            vmem((n_ep, 2, width), BF),
            vmem((n_tp, GROUP * rows, n_z * units), BF),
            vmem((GROUP, rows, span), BF),
            vmem((GROUP, rows, span), BF),
            vmem((n_tp, n_pick, span), BF),
            vmem((n_tp, n_pick, span), BF),
            vmem((n_ep, 2, span), BF),
            vmem((n_ep, 2, span), BF),
            vmem((128, n_pick), BF),
            vmem((128, n_pick), BF),
            vmem((n_pick, 128), BF),
            dma((11,)),
            dma((rows,)),
            dma((8,)),
            dma((3,)),
            dma((3, n_z)),
            dma((3, n_z)),
            dma((n_tp,)),
            dma((n_tp,)),
            dma,
            dma,
            dma((GROUP,)),
            dma((GROUP,)),
            dma((n_tp,)),
            dma((n_tp,)),
            dma((GROUP,)),
            dma((GROUP,)),
            dma((n_tp,)),
            dma((n_tp,)),
            dma,
            dma,
        ]
        return pl.pallas_call(
            functools.partial(kernel, n_ep, n_tp),
            out_shape=jax.ShapeDtypeStruct((rows, span), BF),
            in_specs=[pl.BlockSpec(memory_space=pltpu.HBM)] * len(operands),
            out_specs=pl.BlockSpec(memory_space=pltpu.VMEM),
            scratch_shapes=scratch,
            name="layer",
            compiler_params=pltpu.CompilerParams(
                collective_id=0, has_side_effects=True, vmem_limit_bytes=56 * 1024 * 1024
            ),
        )(*operands)

    return jax.shard_map(
        shards,
        mesh=mesh,
        in_specs=(
            P("ep", None),
            P(),
            P(None, "tp"),
            P(None, "tp"),
            P(None, "tp"),
            P(None, "tp"),
            P("tp"),
            P(),
            P(),
            P("ep", "tp", None, None),
            P("ep", "tp", None),
            P("ep"),
            P("tp", None),
            P(),
            P(),
            P(),
            P("ep", None, "tp"),
            P("ep", None, "tp"),
            P("ep", "tp", None),
            P(),
            P("ep", None),
            P("ep", None),
            P("ep", "tp"),
        ),
        out_specs=P("ep", "tp"),
        check_vma=False,
    )
```

time: 140 us -> 58.7 us (0.42)
  Pallas kernels: 0 us -> 55.3 us
  waiting for transfers between devices: 46.6 us -> 0 us
  matrix products: 25.6 us -> 0 us
  blocking collectives: 25.5 us -> 0 us
  starting transfers between devices: 20.2 us -> 0 us
  other arithmetic: 12.5 us -> 0 us
  local copies, waits for them, and re-layouts: 7.02 us -> 2.59 us
    pallas_call x0 -> x1, Pallas kernels: none -> 55.3 us  [shards(): pl.pallas_call(functools.partial(kernel, n_ep, n_tp), out_shape=jax.Shape...]
    all_to_all x3 -> x0, waiting for transfers between devices: 46.6 us -> none  [the longest x1 31.5 us: from_everyone(): lax.all_to_all(jnp.broadcast_to(x[None], (count, *x.shape)), axis, 0, 0,...]
    dot_general x15 -> x0, matrix products: 25.6 us -> none  [the longest x1 4.76 us: shards(): jnp.einsum('bkgd,bkld->bkgl', query_rows, cached_keys, preferred_element_...]
    all_to_all x3 -> x0, blocking collectives: 25.5 us -> none  [the longest x2 20 us: from_everyone(): lax.all_to_all(jnp.broadcast_to(x[None], (count, *x.shape)), axis, 0, 0,...]
    all_to_all x3 -> x0, starting transfers between devices: 20.2 us -> none  [the longest x1 11.3 us: from_everyone(): lax.all_to_all(jnp.broadcast_to(x[None], (count, *x.shape)), axis, 0, 0,...]
    reduce_sum x11 -> x0, other arithmetic: 5.17 us -> none  [the longest x1 1.33 us: shards(): weight_here = jnp.sum(jnp.where(chosen, route_weight, 0.0), axis=1)]
    another operation x2 -> x0, local copies, waits for them, and re-layouts: 1.87 us -> none  [the longest x1 1.18 us: in_blocks(): x.reshape(*shape[:dim], count, shape[dim] // count, *shape[dim + 1:])]
    sub x2 -> x0, other arithmetic: 1.83 us -> none  [the longest x1 1.03 us: shards(): past_score = past_score + (now_cum[:, :, None] - cache_cum)[:, :, None, :]]
  transfers between devices with their start and end apart: 3 -> 0, of which waited for: 3 -> 0; matrix products, arithmetic and copies ran while one was open for 7% -> 0% of each run, Pallas kernels for 0% -> 0%
where the time goes in v1:
time: 58.7 us; the launch traced here: 58.5 us
  Pallas kernels  55.3 us (94%)
  local copies, waits for them, and re-layouts  2.59 us (4%)
  between operations  0.66 us (1%)
    pallas_call x1, Pallas kernels, shards(): pl.pallas_call(functools.partial(kernel, n_ep, n_tp), out_shape=jax.Shape...  55.3 us
    unnamed x1, local copies, waits for them, and re-layouts  1.31 us
    reshape x1, local copies, waits for them, and re-layouts, shards(): shared_gate.reshape(1, -1)  1.28 us

profile of v1, /device:TPU:1, one launch (start us, length us, event | category | flops | bytes accessed | tf_op | source)
XLA Modules:
  0.0 58.5 jit_solution(10592347974756742259)
XLA Ops:
  0.7 1.3 %reshape.27.shared_gate_h = bf16[1,1024]{1,0:T(2,128)(2,1)} reshape(bf16[1024]{0:T(1024)(128)(2,1)} %param.42) | data formatting | bytes 4096 | tf_op jit(solution)/shard_map/reshape | solution.py:574
  1.9 55.3 %layer.1 = bf16[24,256]{1,0:T(8,128)(2,1)} custom-call(bf16[24,1024]{1,0:T(8,128)(2,1)} %tokens_h.1, f32[1,1024]{1,0:T(1,128)} %bitcast.16, bf16[1024,256]{1,0:T(8,128)(2,1)} %w_query_h.1, bf16[64,1024]{1,0:T(8,128)(2,1)} %bitcast.12, bf16[64,1024]{1,0:T(8,128)(2,1)} %bitcast.13, bf16[1,1024]{1,0:T(2,128)(2,1)} %bitcast.17, f32[1,1]{1,0:T(1,128)} %bitcast.11.forget_bias_h, ...), custom_call_target="tpu_custom_call" | custom-call | tf_op jit(solution)/shard_map/layer/pallas_call | solution.py:645
  57.2 1.3 %copy.26 = bf16[24,256]{1,0:T(8,128)(2,1)} copy(bf16[24,256]{1,0:T(8,128)(2,1)} %layer.1) | data formatting | bytes 24576

commit v2 on v1

--- a/solution.py
+++ b/solution.py
@@ -87,11 +87,11 @@
     wd,
     sg,
     gz,
-    uz,
     dz,
     bias_rows,
     q_rows,
     mix_rows,
+    scores,
     xr,
     resid,
     dt,
@@ -136,7 +136,7 @@
     base = ep - g
     head = qg.shape[1]
     span = width // n_tp
-    units = gz.shape[1]
+    units = gz.shape[2]
 
     def x_peer(k):
         return {"ep": ep, "tp": lax.rem(tp + k, n_tp)}
@@ -163,6 +163,13 @@
     loads = [pltpu.make_async_copy(s, d, load_sem.at[i]) for i, (s, d) in enumerate(small)]
     for c in loads:
         c.start()
+    cache_loads = []
+    for s in range(rows):
+        c = pltpu.make_async_copy(
+            cache_h.at[s, 0], cache.at[s], cache_sem.at[s]
+        )
+        c.start()
+        cache_loads.append(c)
     barrier = pltpu.get_barrier_semaphore()
 
     def greet(k, carry):
@@ -177,13 +184,6 @@
     lax.fori_loop(1, n_ep, greet, 0)
     for k in range(1, n_tp):
         pl.semaphore_signal(barrier, inc=1, device_id=x_peer(k), device_id_type=MESH)
-    cache_loads = []
-    for s in range(rows):
-        c = pltpu.make_async_copy(
-            cache_h.at[s, 0], cache.at[s // 2, :, pl.ds(128 * (s % 2), 128)], cache_sem.at[s]
-        )
-        c.start()
-        cache_loads.append(c)
     later = [
         (w_output_h, wo),
         (ffn_gain_h, fgain),
@@ -199,12 +199,34 @@
         c.start()
     quarter = pl.ds(pl.multiple_of(tp * units, units), units)
     own_dense = [
-        pltpu.make_async_copy(dense_gate_h.at[quarter], gz.at[0], z_local_sem.at[0]),
-        pltpu.make_async_copy(dense_up_h.at[quarter], uz.at[0], z_local_sem.at[1]),
+        pltpu.make_async_copy(dense_gate_h.at[quarter], gz.at[0, 0], z_local_sem.at[0]),
+        pltpu.make_async_copy(dense_up_h.at[quarter], gz.at[0, 1], z_local_sem.at[1]),
         pltpu.make_async_copy(dense_down_h, dz.at[0], z_local_sem.at[2]),
     ]
     for c in own_dense:
         c.start()
+
+    z_copies = {}
+
+    def pass_on(t):
+        for come, go, to in ((t, t + 1, 1), ((n_z - t) % n_z, n_z - 1 - t, n_z - 1)):
+            if (t < n_z // 2) if to == 1 else (t < n_z - 1 - n_z // 2):
+                if t:
+                    for c in z_copies[come]:
+                        c.wait_recv()
+                z_copies[go] = [
+                    pltpu.make_async_remote_copy(
+                        src_ref=held.at[come],
+                        dst_ref=held.at[go],
+                        send_sem=z_send.at[i, go],
+                        recv_sem=z_recv.at[i, go],
+                        device_id=z_peer(to),
+                        device_id_type=MESH,
+                    )
+                    for i, held in enumerate((gz, dz))
+                ]
+                for c in z_copies[go]:
+                    c.start()
 
     for c in loads:
         c.wait()
@@ -261,51 +283,65 @@
     now_cum = last_cum + log_gate
     bias_rows[...] = jnp.where(position < lens_col, now_cum - cum_2d, NEG)
 
-    pl.semaphore_wait(barrier, n_ep - 1 + n_tp - 1)
-    z_copies = []
-    for k in (4, 3, 5, 2, 6, 1, 7):
-        for i, (src, dst) in enumerate(
-            ((dense_gate_h.at[quarter], gz), (dense_up_h.at[quarter], uz), (dense_down_h, dz))
-        ):
-            z_copies.append(
-                pltpu.make_async_remote_copy(
-                    src_ref=src,
-                    dst_ref=dst.at[k],
-                    send_sem=z_send.at[i, k],
-                    recv_sem=z_recv.at[i, k],
-                    device_id=z_peer(k),
-                    device_id_type=MESH,
+    pair = 2 * heads
+    per = 3
+    batches = rows // 2 // per
+    batch_rows = per * pair
+
+    def both_of(p, c):
+        at = pl.ds(256 * c, 256)
+        return jnp.concatenate([cache[2 * p, at, :], cache[2 * p + 1, at, :]], axis=1)
+
+    def score_batch(b):
+        for i in range(2 * per * b, 2 * per * (b + 1)):
+            cache_loads[i].wait()
+        for p in range(per * b, per * (b + 1)):
+            q_pair = q_rows[pl.ds(pair * p, pair), :].astype(BF)
+            for c in range(slots // 256):
+                scores[pl.ds(pair * p, pair), pl.ds(256 * c, 256)] = dot_nt(q_pair, both_of(p, c))
+
+    first = iota((pair, slots), 0) < heads
+    totals = []
+    own_parts = []
+    score_batch(0)
+    for b in range(batches):
+        if b + 1 < batches:
+            score_batch(b + 1)
+        if b == 1:
+            pl.semaphore_wait(barrier, n_ep - 1 + n_tp - 1)
+            for c in own_dense:
+                c.wait()
+            pass_on(0)
+        decay = jnp.concatenate(
+            [
+                jnp.where(
+                    first,
+                    jnp.broadcast_to(bias_rows[pl.ds(2 * p, 1), :], (pair, slots)),
+                    jnp.broadcast_to(bias_rows[pl.ds(2 * p + 1, 1), :], (pair, slots)),
                 )
-            )
-    for c in z_copies:
-        c.start()
-
-    pair = 2 * heads
-    first = iota((pair, slots), 0) < heads
-    own_probs = []
-    for p in range(rows // 2):
-        cache_loads[2 * p].wait()
-        cache_loads[2 * p + 1].wait()
-        q_pair = q_rows[pl.ds(pair * p, pair), :].astype(BF)
-        score = jnp.concatenate(
-            [dot_nt(q_pair, cache[p, pl.ds(256 * c, 256), :]) for c in range(slots // 256)], axis=1
+                for p in range(per * b, per * (b + 1))
+            ],
+            axis=0,
         )
-        decay = jnp.where(
-            first,
-            jnp.broadcast_to(bias_rows[pl.ds(2 * p, 1), :], (pair, slots)),
-            jnp.broadcast_to(bias_rows[pl.ds(2 * p + 1, 1), :], (pair, slots)),
-        )
-        score = score + decay
-        own = own_score[pair * p : pair * (p + 1)]
+        here = pl.ds(batch_rows * b, batch_rows)
+        score = scores[here, :] + decay
+        own = own_score[batch_rows * b : batch_rows * (b + 1)]
         peak = jnp.maximum(jnp.max(score, axis=1, keepdims=True), own)
         past = jnp.exp(score - peak)
         own_exp = jnp.exp(own - peak)
-        inverse = 1.0 / (jnp.sum(past, axis=1, keepdims=True) + own_exp)
-        prob = (past * inverse).astype(BF)
-        own_probs.append((own_exp * inverse).astype(BF).astype(F32))
-        mix_rows[pl.ds(pair * p, pair), :] = dot(prob, cache[p])
+        totals.append(jnp.sum(past, axis=1, keepdims=True) + own_exp)
+        own_parts.append(own_exp)
+        prob = past.astype(BF)
+        for i in range(per):
+            p = per * b + i
+            prob_pair = prob[pair * i : pair * (i + 1)]
+            total = dot(prob_pair[:, :256], both_of(p, 0))
+            for c in range(1, slots // 256):
+                total = total + dot(prob_pair[:, 256 * c : 256 * (c + 1)], both_of(p, c))
+            mix_rows[pl.ds(pair * p, pair), :] = total
+    inverse = 1.0 / jnp.concatenate(totals, axis=0)
     mixed = jnp.where(high, mix_rows[...], 0.0)
-    mixed = mixed + jnp.concatenate(own_probs, axis=0) * value_wide
+    mixed = (mixed + jnp.concatenate(own_parts, axis=0) * value_wide) * inverse
     by_head = jnp.where(own_head, dot(mixed.astype(BF), fold), 0.0).astype(BF)
     to_seq = one_hot(iota((rows, n_rows), 1) // heads == iota((rows, n_rows), 0))
     head_mix = dot(to_seq, by_head).astype(BF)
@@ -324,6 +360,8 @@
         )
         c.start()
         x_copies.append(c)
+
+    pass_on(1)
 
     n_pick = 2 * n_ep
     tokens_all = ids.shape[1]
@@ -359,7 +397,9 @@
     resid[...] = residual
     normed_two = (residual * rms(residual) * fgain[...]).astype(BF)
     dt[0] = normed_two
-    mix_gate = jnp.sum(normed_two.astype(F32) * sg[...].astype(F32), axis=1, keepdims=True)
+    gate_row = sg[...].astype(F32)
+    gate_row = jnp.concatenate([gate_row[i : i + 1] for i in range(width // 128)], axis=1)
+    mix_gate = jnp.sum(normed_two.astype(F32) * gate_row, axis=1, keepdims=True)
     mix_gate = 1.0 / (1.0 + jnp.exp(-mix_gate))
     packed = dot(pick[:, :rows], normed_two).astype(BF)
     send_rows[...] = packed.reshape(n_ep, 2, width)
@@ -390,6 +430,9 @@
         )
         c.start()
         t_copies.append(c)
+
+    pass_on(2)
+    pass_on(3)
 
     for c in late_loads[5:]:
         c.wait()
@@ -421,16 +464,15 @@
             c.start()
             e_copies.append(c)
 
-    for c in own_dense:
-        c.wait()
-    for c in z_copies:
-        c.wait_recv()
+    for come in (n_z // 2, n_z - (n_z - 1 - n_z // 2)):
+        for c in z_copies[come]:
+            c.wait_recv()
     for c in t_copies:
         c.wait_recv()
     group_rows = dt[...].reshape(GROUP * rows, width)
     dense_w = n_z * units
-    dense_gate = dot_nt(group_rows, gz[...].reshape(dense_w, width))
-    dense_up = dot_nt(group_rows, uz[...].reshape(dense_w, width))
+    dense_gate = dot_nt(group_rows, gz[:, 0].reshape(dense_w, width))
+    dense_up = dot_nt(group_rows, gz[:, 1].reshape(dense_w, width))
     hx[0] = (silu(dense_gate) * dense_up).astype(BF)
     h_copies = []
     for k in (2, 1, 3):
@@ -507,7 +549,7 @@
     out = resid[:, mine_cols] + expert_sum[:rows] + mix_gate * dense_sum
     out_ref[...] = out.astype(BF)
 
-    for c in z_copies + x_copies + t_copies + e_copies + h_copies + d_copies:
+    for c in sum(z_copies.values(), []) + x_copies + t_copies + e_copies + h_copies + d_copies:
         c.wait_send()
     arrivals.wait_send()
     returned.wait_send()
@@ -571,7 +613,7 @@
             w_exp_gate,
             w_exp_up,
             w_exp_down,
-            shared_gate.reshape(1, -1),
+            shared_gate.reshape(-1, 128),
             w_dense_gate,
             w_dense_up,
             w_dense_down,
@@ -589,7 +631,7 @@
             like(operands[6]),
             like(operands[7]),
             like(operands[8]),
-            vmem((rows // 2, slots, 256), BF),
+            vmem((rows, slots, 128), BF),
             like(cache_cum),
             like(operands[11]),
             like(w_output),
@@ -600,12 +642,12 @@
             vmem((width, ff), BF),
             vmem((ff, width), BF),
             like(operands[19]),
-            vmem((n_z, units, width), BF),
-            vmem((n_z, units, width), BF),
+            vmem((n_z, 2, units, width), BF),
             vmem((n_z, units * n_tp, span), BF),
             vmem((rows, slots), F32),
             vmem((n_rows, 256), F32),
             vmem((n_rows, 256), F32),
+            vmem((n_rows, slots), F32),
             vmem((n_tp, rows, width), BF),
             vmem((rows, width), F32),
             vmem((GROUP, rows, width), BF),
@@ -625,8 +667,8 @@
             dma((rows,)),
             dma((8,)),
             dma((3,)),
-            dma((3, n_z)),
-            dma((3, n_z)),
+            dma((2, n_z)),
+            dma((2, n_z)),
             dma((n_tp,)),
             dma((n_tp,)),
             dma,

time: 58.7 us -> 48 us (0.82)
  Pallas kernels: 55.3 us -> 45.9 us
  local copies, waits for them, and re-layouts: 2.59 us -> 1.31 us
    pallas_call x1, Pallas kernels: 55.3 us -> 45.9 us  [shards(): pl.pallas_call(functools.partial(kernel, n_ep, n_tp), out_shape=jax.Shape...]
    reshape x1 -> x0, local copies, waits for them, and re-layouts: 1.28 us -> none  [shards(): shared_gate.reshape(1, -1)]
where the time goes in v2:
time: 48 us; the launch traced here: 47.9 us
  Pallas kernels  45.9 us (96%)
  local copies, waits for them, and re-layouts  1.31 us (3%)
  between operations  0.66 us (1%)
    pallas_call x1, Pallas kernels, shards(): pl.pallas_call(functools.partial(kernel, n_ep, n_tp), out_shape=jax.Shape...  45.9 us
    unnamed x1, local copies, waits for them, and re-layouts  1.31 us

profile of v2, /device:TPU:1, one launch (start us, length us, event | category | flops | bytes accessed | tf_op | source)
XLA Modules:
  0.0 47.9 jit_solution(2318314083719144640)
XLA Ops:
  0.7 45.9 %layer.1 = bf16[24,256]{1,0:T(8,128)(2,1)} custom-call(bf16[24,1024]{1,0:T(8,128)(2,1)} %tokens_h.1, f32[1,1024]{1,0:T(1,128)} %bitcast.17, bf16[1024,256]{1,0:T(8,128)(2,1)} %w_query_h.1, bf16[64,1024]{1,0:T(8,128)(2,1)} %bitcast.13, bf16[64,1024]{1,0:T(8,128)(2,1)} %bitcast.14, bf16[1,1024]{1,0:T(2,128)(2,1)} %bitcast.18, f32[1,1]{1,0:T(1,128)} %bitcast.12.forget_bias_h, ...), custom_call_target="tpu_custom_call" | custom-call | tf_op jit(solution)/shard_map/layer/pallas_call | solution.py:687
  46.6 1.3 %copy.26 = bf16[24,256]{1,0:T(8,128)(2,1)} copy(bf16[24,256]{1,0:T(8,128)(2,1)} %layer.1) | data formatting | bytes 24576

commit v3 on v2

--- a/solution.py
+++ b/solution.py
@@ -138,6 +138,41 @@
     span = width // n_tp
     units = gz.shape[2]
 
+    z = ep // GROUP
+    far_first = [n_z // 2]
+    for k in range(1, n_z // 2):
+        far_first += [n_z // 2 - k, n_z // 2 + k]
+    far_first += [0]
+    parts = 2
+    part_z = n_z // parts
+    part_slots = n_ep // parts
+
+    def ep_peer(far, low):
+        return lax.rem(z + far, n_z) * GROUP + lax.rem(g + low, GROUP)
+
+    def exchange(half, source, target, send_sem, recv_sem, back):
+        for i in range(part_z * half, part_z * (half + 1)):
+            far = far_first[i]
+
+            def one(low, carry):
+                if back:
+                    to = ep_peer(n_z - far, GROUP - low)
+                else:
+                    to = ep_peer(far, low)
+                pltpu.make_async_remote_copy(
+                    src_ref=source.at[GROUP * i + low],
+                    dst_ref=target.at[GROUP * i + low],
+                    send_sem=send_sem,
+                    recv_sem=recv_sem,
+                    device_id={"ep": to, "tp": tp},
+                    device_id_type=MESH,
+                ).start()
+                return carry
+
+            lax.fori_loop(0 if far else 1, GROUP, one, 0)
+
+    own_slot = n_ep - GROUP
+
     def x_peer(k):
         return {"ep": ep, "tp": lax.rem(tp + k, n_tp)}
 
@@ -195,7 +230,7 @@
         (w_down_h.at[0], wd),
     ]
     late_loads = [pltpu.make_async_copy(s, d, weight_sem.at[i]) for i, (s, d) in enumerate(later)]
-    for c in late_loads:
+    for c in late_loads[:5]:
         c.start()
     quarter = pl.ds(pl.multiple_of(tp * units, units), units)
     own_dense = [
@@ -308,6 +343,8 @@
         if b + 1 < batches:
             score_batch(b + 1)
         if b == 1:
+            for c in late_loads[5:]:
+                c.start()
             pl.semaphore_wait(barrier, n_ep - 1 + n_tp - 1)
             for c in own_dense:
                 c.wait()
@@ -375,7 +412,12 @@
     both = jnp.concatenate([ids[:, lanes].astype(F32), route[:, lanes]], axis=0)
     mine = jnp.dot(both, pick_lanes, precision=lax.Precision.HIGHEST, preferred_element_type=F32)
     lane_p = iota((n_pick, 128), 1)
-    expert = (iota((n_pick, 128), 0) // 2).astype(F32)
+    slot_of = iota((n_pick, 128), 0) // 2
+    far_of = jnp.zeros((n_pick, 128), jnp.int32)
+    for i, far in enumerate(far_first):
+        far_of = jnp.where(slot_of // GROUP == i, far, far_of)
+    expert = lax.rem(z + far_of, n_z) * GROUP + lax.rem(g + slot_of % GROUP, GROUP)
+    expert = expert.astype(F32)
     live = lane_p < rows
     hit_0 = (mine[0:1] == expert) & live
     hit_1 = (mine[1:2] == expert) & live
@@ -401,23 +443,12 @@
     gate_row = jnp.concatenate([gate_row[i : i + 1] for i in range(width // 128)], axis=1)
     mix_gate = jnp.sum(normed_two.astype(F32) * gate_row, axis=1, keepdims=True)
     mix_gate = 1.0 / (1.0 + jnp.exp(-mix_gate))
-    packed = dot(pick[:, :rows], normed_two).astype(BF)
-    send_rows[...] = packed.reshape(n_ep, 2, width)
-    recv_rows[ep] = send_rows[ep]
-
-    def dispatch(k, carry):
-        to = lax.rem(ep + k, n_ep)
-        pltpu.make_async_remote_copy(
-            src_ref=send_rows.at[to],
-            dst_ref=recv_rows.at[ep],
-            send_sem=a_send,
-            recv_sem=a_recv,
-            device_id={"ep": to, "tp": tp},
-            device_id_type=MESH,
-        ).start()
-        return carry
-
-    lax.fori_loop(1, n_ep, dispatch, 0)
+    for half in range(parts):
+        at = pl.ds(2 * part_slots * half, 2 * part_slots)
+        packed = dot(pick[at, :rows], normed_two).astype(BF)
+        send_rows[pl.ds(part_slots * half, part_slots)] = packed.reshape(part_slots, 2, width)
+        exchange(half, send_rows, recv_rows, a_send, a_recv, False)
+    recv_rows[own_slot] = send_rows[own_slot]
     t_copies = []
     for k in range(1, GROUP):
         c = pltpu.make_async_remote_copy(
@@ -448,21 +479,25 @@
     arrivals.wait_recv()
     routed = recv_rows[...].reshape(n_pick, width)
     hidden = (silu(dot(routed, wg[...])) * dot(routed, wu[...])).astype(BF)
-    e_copies = []
+    e_copies = [[], []]
     for k in (2, 1, 3, 0):
         column = pl.ds(pl.multiple_of(lax.rem(tp + k, n_tp) * span, span), span)
-        esend[k] = dot(hidden, wd[:, column]).astype(BF)
+        part = dot(hidden, wd[:, column]).astype(BF)
+        esend[k] = part.reshape(parts, n_pick // parts, span)
         if k:
-            c = pltpu.make_async_remote_copy(
-                src_ref=esend.at[k],
-                dst_ref=erecv.at[k],
-                send_sem=e_send.at[k],
-                recv_sem=e_recv.at[k],
-                device_id=x_peer(k),
-                device_id_type=MESH,
-            )
-            c.start()
-            e_copies.append(c)
+            for half in range(parts):
+                c = pltpu.make_async_remote_copy(
+                    src_ref=esend.at[k, half],
+                    dst_ref=erecv.at[k, half],
+                    send_sem=e_send.at[k, half],
+                    recv_sem=e_recv.at[k, half],
+                    device_id=x_peer(k),
+                    device_id_type=MESH,
+                )
+                e_copies[half].append(c)
+            e_copies[0][-1].start()
+    for c in e_copies[1]:
+        c.start()
 
     for come in (n_z // 2, n_z - (n_z - 1 - n_z // 2)):
         for c in z_copies[come]:
@@ -487,26 +522,15 @@
         c.start()
         h_copies.append(c)
 
-    for c in e_copies:
-        c.wait_recv()
-    summed = esend[0].astype(F32) + erecv[1].astype(F32) + erecv[2].astype(F32)
-    summed = (summed + erecv[3].astype(F32)).astype(BF)
-    back_send[...] = summed.reshape(n_ep, 2, span)
-    back_recv[ep] = back_send[ep]
-
-    def give_back(k, carry):
-        to = lax.rem(ep + k, n_ep)
-        pltpu.make_async_remote_copy(
-            src_ref=back_send.at[to],
-            dst_ref=back_recv.at[ep],
-            send_sem=b_send,
-            recv_sem=b_recv,
-            device_id={"ep": to, "tp": tp},
-            device_id_type=MESH,
-        ).start()
-        return carry
-
-    lax.fori_loop(1, n_ep, give_back, 0)
+    for half in range(parts):
+        for c in e_copies[half]:
+            c.wait_recv()
+        summed = esend[0, half].astype(F32) + erecv[1, half].astype(F32)
+        summed = summed + erecv[2, half].astype(F32) + erecv[3, half].astype(F32)
+        at = pl.ds(part_slots * half, part_slots)
+        back_send[at] = summed.astype(BF).reshape(part_slots, 2, span)
+        exchange(half, back_send, back_recv, b_send, b_recv, True)
+    back_recv[own_slot] = back_send[own_slot]
 
     for c in h_copies:
         c.wait_recv()
@@ -549,7 +573,7 @@
     out = resid[:, mine_cols] + expert_sum[:rows] + mix_gate * dense_sum
     out_ref[...] = out.astype(BF)
 
-    for c in sum(z_copies.values(), []) + x_copies + t_copies + e_copies + h_copies + d_copies:
+    for c in sum(z_copies.values(), []) + x_copies + t_copies + sum(e_copies, []) + h_copies + d_copies:
         c.wait_send()
     arrivals.wait_send()
     returned.wait_send()
@@ -656,8 +680,8 @@
             vmem((n_tp, GROUP * rows, n_z * units), BF),
             vmem((GROUP, rows, span), BF),
             vmem((GROUP, rows, span), BF),
-            vmem((n_tp, n_pick, span), BF),
-            vmem((n_tp, n_pick, span), BF),
+            vmem((n_tp, 2, n_ep, span), BF),
+            vmem((n_tp, 2, n_ep, span), BF),
             vmem((n_ep, 2, span), BF),
             vmem((n_ep, 2, span), BF),
             vmem((128, n_pick), BF),
@@ -679,14 +703,14 @@
             dma((n_tp,)),
             dma((GROUP,)),
             dma((GROUP,)),
-            dma((n_tp,)),
-            dma((n_tp,)),
+            dma((n_tp, 2)),
+            dma((n_tp, 2)),
             dma,
             dma,
         ]
         return pl.pallas_call(
             functools.partial(kernel, n_ep, n_tp),
-            out_shape=jax.ShapeDtypeStruct((rows, span), BF),
+            out_shape=pltpu.VMEM((rows, span), BF),
             in_specs=[pl.BlockSpec(memory_space=pltpu.HBM)] * len(operands),
             out_specs=pl.BlockSpec(memory_space=pltpu.VMEM),
             scratch_shapes=scratch,

time: 48 us -> 44.6 us (0.929)
  Pallas kernels: 45.9 us -> 43.3 us
  local copies, waits for them, and re-layouts: 1.31 us -> 0.6 us
    pallas_call x1, Pallas kernels: 45.9 us -> 43.3 us  [shards(): pl.pallas_call(functools.partial(kernel, n_ep, n_tp), out_shape=pltpu.VME...]
    unnamed x1, local copies, waits for them, and re-layouts: 1.31 us -> 0.6 us
where the time goes in v3:
time: 44.6 us; the launch traced here: 44.5 us
  Pallas kernels  43.3 us (97%)
  between operations  0.66 us (1%)
  local copies, waits for them, and re-layouts  0.6 us (1%)
    pallas_call x1, Pallas kernels, shards(): pl.pallas_call(functools.partial(kernel, n_ep, n_tp), out_shape=pltpu.VME...  43.3 us

profile of v3, /device:TPU:1, one launch (start us, length us, event | category | flops | bytes accessed | tf_op | source)
XLA Modules:
  0.0 44.5 jit_solution(6659673096477721119)
XLA Ops:
  0.7 43.3 %layer.1 = bf16[24,256]{1,0:T(8,128)(2,1)S(1)} custom-call(bf16[24,1024]{1,0:T(8,128)(2,1)} %tokens_h.1, f32[1,1024]{1,0:T(1,128)} %bitcast.17, bf16[1024,256]{1,0:T(8,128)(2,1)} %w_query_h.1, bf16[64,1024]{1,0:T(8,128)(2,1)} %bitcast.13, bf16[64,1024]{1,0:T(8,128)(2,1)} %bitcast.14, bf16[1,1024]{1,0:T(2,128)(2,1)} %bitcast.18, ...), custom_call_target="tpu_custom_call" | custom-call | tf_op jit(solution)/shard_map/layer/pallas_call | solution.py:711
  43.9 0.6 %copy.25 = bf16[24,256]{1,0:T(8,128)(2,1)} copy(bf16[24,256]{1,0:T(8,128)(2,1)S(1)} %layer.1) | data formatting | bytes 24576

commit v4 on v3

--- a/solution.py
+++ b/solution.py
@@ -198,6 +198,15 @@
     loads = [pltpu.make_async_copy(s, d, load_sem.at[i]) for i, (s, d) in enumerate(small)]
     for c in loads:
         c.start()
+    quarter = pl.ds(pl.multiple_of(tp * units, units), units)
+    own_dense = [
+        pltpu.make_async_copy(dense_gate_h.at[quarter], gz.at[0, 0], z_local_sem.at[0]),
+        pltpu.make_async_copy(dense_up_h.at[quarter], gz.at[0, 1], z_local_sem.at[1]),
+        pltpu.make_async_copy(dense_down_h, dz.at[0], z_local_sem.at[2]),
+    ]
+    for c in own_dense:
+        c.start()
+
     cache_loads = []
     for s in range(rows):
         c = pltpu.make_async_copy(
@@ -232,15 +241,6 @@
     late_loads = [pltpu.make_async_copy(s, d, weight_sem.at[i]) for i, (s, d) in enumerate(later)]
     for c in late_loads[:5]:
         c.start()
-    quarter = pl.ds(pl.multiple_of(tp * units, units), units)
-    own_dense = [
-        pltpu.make_async_copy(dense_gate_h.at[quarter], gz.at[0, 0], z_local_sem.at[0]),
-        pltpu.make_async_copy(dense_up_h.at[quarter], gz.at[0, 1], z_local_sem.at[1]),
-        pltpu.make_async_copy(dense_down_h, dz.at[0], z_local_sem.at[2]),
-    ]
-    for c in own_dense:
-        c.start()
-
     z_copies = {}
 
     def pass_on(t):
@@ -319,7 +319,7 @@
     bias_rows[...] = jnp.where(position < lens_col, now_cum - cum_2d, NEG)
 
     pair = 2 * heads
-    per = 3
+    per = 6
     batches = rows // 2 // per
     batch_rows = per * pair
 
@@ -339,16 +339,16 @@
     totals = []
     own_parts = []
     score_batch(0)
+    pl.semaphore_wait(barrier, n_ep - 1 + n_tp - 1)
+    for c in own_dense:
+        c.wait()
+    pass_on(0)
     for b in range(batches):
         if b + 1 < batches:
             score_batch(b + 1)
-        if b == 1:
+        if b == 0:
             for c in late_loads[5:]:
                 c.start()
-            pl.semaphore_wait(barrier, n_ep - 1 + n_tp - 1)
-            for c in own_dense:
-                c.wait()
-            pass_on(0)
         decay = jnp.concatenate(
             [
                 jnp.where(

time: 44.6 us -> 43.8 us (0.982)
  Pallas kernels: 43.3 us -> 42.5 us
    pallas_call x1, Pallas kernels: 43.3 us -> 42.5 us  [shards(): pl.pallas_call(functools.partial(kernel, n_ep, n_tp), out_shape=pltpu.VME...]
where the time goes in v4:
time: 43.8 us; the launch traced here: 43.7 us
  Pallas kernels  42.5 us (97%)
  between operations  0.66 us (2%)
  local copies, waits for them, and re-layouts  0.6 us (1%)
    pallas_call x1, Pallas kernels, shards(): pl.pallas_call(functools.partial(kernel, n_ep, n_tp), out_shape=pltpu.VME...  42.5 us

profile of v4, /device:TPU:1, one launch (start us, length us, event | category | flops | bytes accessed | tf_op | source)
XLA Modules:
  0.0 43.7 jit_solution(11586284516137965543)
XLA Ops:
  0.7 42.5 %layer.1 = bf16[24,256]{1,0:T(8,128)(2,1)S(1)} custom-call(bf16[24,1024]{1,0:T(8,128)(2,1)} %tokens_h.1, f32[1,1024]{1,0:T(1,128)} %bitcast.17, bf16[1024,256]{1,0:T(8,128)(2,1)} %w_query_h.1, bf16[64,1024]{1,0:T(8,128)(2,1)} %bitcast.13, bf16[64,1024]{1,0:T(8,128)(2,1)} %bitcast.14, bf16[1,1024]{1,0:T(2,128)(2,1)} %bitcast.18, ...), custom_call_target="tpu_custom_call" | custom-call | tf_op jit(solution)/shard_map/layer/pallas_call | solution.py:711
  43.1 0.6 %copy.25 = bf16[24,256]{1,0:T(8,128)(2,1)} copy(bf16[24,256]{1,0:T(8,128)(2,1)S(1)} %layer.1) | data formatting | bytes 24576

commit v5 on v4

--- a/solution.py
+++ b/solution.py
@@ -398,8 +398,6 @@
         c.start()
         x_copies.append(c)
 
-    pass_on(1)
-
     n_pick = 2 * n_ep
     tokens_all = ids.shape[1]
     window = 256
@@ -432,6 +430,7 @@
     comb_hi[...] = combine_hi
     comb_lo[...] = (combine - combine_hi.astype(F32)).astype(BF)
 
+    pass_on(1)
     for c in x_copies:
         c.wait_recv()
     attn_out = xr[0].astype(F32) + xr[1].astype(F32) + xr[2].astype(F32) + xr[3].astype(F32)
@@ -568,9 +567,9 @@
     )
     returned.wait_recv()
     expert_rows = back_recv[...].reshape(n_pick, span)
-    expert_sum = dot(comb_hi[...], expert_rows) + dot(comb_lo[...], expert_rows)
+    expert_sum = dot(comb_hi[:rows], expert_rows) + dot(comb_lo[:rows], expert_rows)
     mine_cols = pl.ds(pl.multiple_of(tp * span, span), span)
-    out = resid[:, mine_cols] + expert_sum[:rows] + mix_gate * dense_sum
+    out = resid[:, mine_cols] + expert_sum + mix_gate * dense_sum
     out_ref[...] = out.astype(BF)
 
     for c in sum(z_copies.values(), []) + x_copies + t_copies + sum(e_copies, []) + h_copies + d_copies:

time: 43.8 us -> 43.8 us (level)
  no operation moved by 1% of the time
where the time goes in v5:
time: 43.8 us; the launch traced here: 43.7 us
  Pallas kernels  42.4 us (97%)
  between operations  0.66 us (2%)
  local copies, waits for them, and re-layouts  0.6 us (1%)
    pallas_call x1, Pallas kernels, shards(): pl.pallas_call(functools.partial(kernel, n_ep, n_tp), out_shape=pltpu.VME...  42.4 us

profile of v5, /device:TPU:1, one launch (start us, length us, event | category | flops | bytes accessed | tf_op | source)
XLA Modules:
  0.0 43.7 jit_solution(1814268318649138426)
XLA Ops:
  0.7 42.4 %layer.1 = bf16[24,256]{1,0:T(8,128)(2,1)S(1)} custom-call(bf16[24,1024]{1,0:T(8,128)(2,1)} %tokens_h.1, f32[1,1024]{1,0:T(1,128)} %bitcast.17, bf16[1024,256]{1,0:T(8,128)(2,1)} %w_query_h.1, bf16[64,1024]{1,0:T(8,128)(2,1)} %bitcast.13, bf16[64,1024]{1,0:T(8,128)(2,1)} %bitcast.14, bf16[1,1024]{1,0:T(2,128)(2,1)} %bitcast.18, ...), custom_call_target="tpu_custom_call" | custom-call | tf_op jit(solution)/shard_map/layer/pallas_call | solution.py:710
  43.1 0.6 %copy.25 = bf16[24,256]{1,0:T(8,128)(2,1)} copy(bf16[24,256]{1,0:T(8,128)(2,1)S(1)} %layer.1) | data formatting | bytes 24576
